TPU v7x, 512 devices: a whole 4x8x8 slice. The times are simulated.
512 devices in a mesh: ep: 128 (over z, y, core), tp: 4 (over x).
Axes of the slice: x: 4, y: 8, z: 8, core: 2. Of those that a mesh axis runs over, the one named last changes fastest.
Arguments:
- tokens: bfloat16 [2048, 1024], P('ep'), may hold values from -24 to 24
- seq_length: int32 [2048], P('ep'), may hold values from 1024 to 16383
- ret_state: float32 [2048, 4, 128, 256], P('ep', 'tp'), may hold values from -0.6 to 0.6
- norm_in: float32 [1024], replicated, may hold values from 0.1 to 1.9
- w_query: bfloat16 [1024, 512], P(None, 'tp'), may hold values from -0.1875 to 0.1875
- w_key: bfloat16 [1024, 512], P(None, 'tp'), may hold values from -0.1875 to 0.1875
- w_value: bfloat16 [1024, 1024], P(None, 'tp'), may hold values from -0.1875 to 0.1875
- head_gain: float32 [1024], P('tp'), may hold values from 0.1 to 1.9
- w_output: bfloat16 [1024, 1024], P('tp'), may hold values from -0.1875 to 0.1875
- norm_mid: float32 [1024], replicated, may hold values from 0.1 to 1.9
- route_expert: int32 [2048, 2], P('ep'), may hold values from 0 to 63, all different within a row; in each aligned block of 16 rows (0 to 15, 16 to 31, ...) at most 2 rows name the same one
- route_score: float32 [2048, 2], P('ep'), may hold values from -6 to 6
- expert_gate: bfloat16 [128, 1024, 1792], P('ep', None, 'tp'), may hold values from -0.1875 to 0.1875
- expert_up: bfloat16 [128, 1024, 1792], P('ep', None, 'tp'), may hold values from -0.1875 to 0.1875
- expert_down: bfloat16 [128, 1792, 1024], P('ep', 'tp'), may hold values from -0.09375 to 0.09375
Outputs:
- mixed: bfloat16 [2048, 1024], P('ep', 'tp')
Inputs may be any that keep to these rules, and one draw needn't show every extreme that they name: `route_expert`: each row names 2 different experts; within the rows of one device no expert is named by more than 2 rows, and some device's rows name one expert exactly 2 times.
All inputs are finite; a program needn't handle non-finite values.
Results may differ from a plain program's by a relative error of at most 0.014.
Values may be sent and summed in bfloat16 or wider, within the bound.
A program may use at most 64 MiB of HBM per device.

v0:
```python
import jax
import jax.numpy as jnp
from jax import lax
from jax.sharding import PartitionSpec as P

DK = 128
DV = 256
SPREAD = 2
TOP_K = 2
EPS = 1e-06


def in_blocks(x, dim, devices):
    lengths = x.shape
    pieces = x.reshape(*lengths[:dim], devices, lengths[dim] // devices, *lengths[dim + 1 :])
    return jnp.moveaxis(pieces, dim, 0)


def summed_on_arrival(x, axis, dim):
    pieces = in_blocks(x, dim, lax.axis_size(axis))
    arrived = lax.all_to_all(pieces, axis, split_axis=0, concat_axis=0, tiled=True)
    return arrived.astype(jnp.float32).sum(axis=0)


def copy_for_each(x, axis):
    copies = jnp.broadcast_to(x, (lax.axis_size(axis), *x.shape))
    return lax.all_to_all(copies, axis, split_axis=0, concat_axis=0, tiled=True)


def over_copies(x, axis):
    return copy_for_each(x, axis).astype(jnp.float32).sum(axis=0)


def rotate(head_rows, positions):
    half_width = head_rows.shape[-1] // 2
    inverse = 10000.0 ** (-jnp.arange(half_width, dtype=jnp.float32) / half_width)
    angles = positions[:, None] * inverse[None, :]
    cosine = jnp.cos(angles)[:, None, :]
    sine_part = jnp.sin(angles)[:, None, :]
    first_half = head_rows[..., :half_width]
    second = head_rows[..., half_width:]
    return jnp.concatenate(
        [first_half * cosine - second * sine_part, first_half * sine_part + second * cosine],
        axis=-1,
    )


def body(
    tokens,
    seq_length,
    ret_state,
    norm_in,
    w_query,
    w_key,
    w_value,
    head_gain,
    w_output,
    norm_mid,
    route_expert,
    route_score,
    expert_gate,
    expert_up,
    expert_down,
):
    n_lanes = lax.axis_size("tp")
    n_groups = lax.axis_size("ep")
    lane_index = lax.axis_index("tp")
    local_rows = tokens.shape[0]
    width = tokens.shape[1]
    quarter = width // n_lanes
    heads_here = w_query.shape[1] // DK
    token_f = tokens.astype(jnp.float32)
    normed = (
        token_f * lax.rsqrt(jnp.mean(token_f * token_f, axis=-1, keepdims=True) + EPS) * norm_in
    ).astype(jnp.bfloat16)
    query_proj = jnp.dot(normed, w_query, preferred_element_type=jnp.float32).astype(jnp.bfloat16)
    key_proj = jnp.dot(normed, w_key, preferred_element_type=jnp.float32).astype(jnp.bfloat16)
    value_proj = jnp.dot(normed, w_value, preferred_element_type=jnp.float32).astype(jnp.bfloat16)
    positions = seq_length.astype(jnp.float32)
    q_rot = rotate(query_proj.astype(jnp.float32).reshape(local_rows, heads_here, DK), positions)
    k_rot = rotate(
        key_proj.astype(jnp.float32).reshape(local_rows, heads_here, DK), positions
    ) * DK ** (-0.5)
    value_rows = value_proj.astype(jnp.float32).reshape(local_rows, heads_here, DV)
    head_index = (lane_index * heads_here + jnp.arange(heads_here, dtype=jnp.int32)).astype(
        jnp.float32
    )
    decay_rate = 1.0 - jnp.exp2(-2.0 - 2.0 * head_index)
    carried = jnp.einsum("bhd,bhde->bhe", q_rot, ret_state)
    within = jnp.sum(q_rot * k_rot, axis=-1, keepdims=True) * value_rows
    retained = decay_rate[None, :, None] * carried + within
    centre = jnp.mean(retained, axis=-1, keepdims=True)
    variance = jnp.mean(jnp.square(retained - centre), axis=-1, keepdims=True)
    ret_out = ((retained - centre) * lax.rsqrt(variance + EPS)).reshape(local_rows, heads_here * DV)
    ret_out = (ret_out * head_gain).astype(jnp.bfloat16)
    partial_value = jnp.dot(ret_out, w_output, preferred_element_type=jnp.float32)
    experts_n = n_groups // SPREAD
    cap = min(local_rows, max(2, 3 * local_rows * TOP_K // (2 * experts_n)))
    flat_rows = route_expert.reshape(-1)
    onehot = (flat_rows[:, None] == jnp.arange(experts_n, dtype=jnp.int32)[None, :]).astype(
        jnp.int32
    )
    rank_index = jnp.sum((jnp.cumsum(onehot, axis=0) - onehot) * onehot, axis=1)
    slot_index = flat_rows * cap + rank_index
    chosen_slot = (
        slot_index[:, None] == jnp.arange(experts_n * cap, dtype=jnp.int32)[None, :]
    ).astype(jnp.float32)
    chosen_slot = chosen_slot.reshape(local_rows, TOP_K, experts_n * cap)
    placing = jnp.sum(chosen_slot, axis=1).astype(jnp.bfloat16)
    weights = jax.nn.softmax(route_score, axis=-1)
    combine = jnp.sum(chosen_slot * weights[:, :, None], axis=1)
    gate_rows = expert_gate[0]
    up_rows = expert_up[0]
    down_rows = expert_down[0]
    attended = over_copies(partial_value.astype(jnp.bfloat16), "tp").astype(jnp.float32)
    resid_full = (token_f + attended).astype(jnp.bfloat16)
    resid_f = resid_full.astype(jnp.float32)
    mid_full = (
        resid_f * lax.rsqrt(jnp.mean(resid_f * resid_f, axis=-1, keepdims=True) + EPS) * norm_mid
    ).astype(jnp.bfloat16)
    resid = lax.dynamic_slice_in_dim(resid_full, lane_index * quarter, quarter, 1)
    mid = lax.dynamic_slice_in_dim(mid_full, lane_index * quarter, quarter, 1)
    packed = jnp.einsum("re,rc->ec", placing, mid, preferred_element_type=jnp.float32).astype(
        jnp.bfloat16
    )
    packed = packed.reshape(experts_n, cap, quarter)
    send_buffer = jnp.repeat(packed, SPREAD, axis=0)
    received = lax.all_to_all(send_buffer, "ep", split_axis=0, concat_axis=0, tiled=True)
    groups, row_count, cols = received.shape
    piece_cols = lax.all_gather(received, "tp", axis=2, tiled=True)
    piece_width = piece_cols.shape[2]
    flat_in = piece_cols.reshape(groups * row_count, piece_width)
    gate_sum = jnp.dot(flat_in, gate_rows, preferred_element_type=jnp.float32)
    up_sum = jnp.dot(flat_in, up_rows, preferred_element_type=jnp.float32)
    hidden = (jax.nn.silu(gate_sum) * up_sum).astype(jnp.bfloat16)
    down_part = jnp.dot(hidden, down_rows, preferred_element_type=jnp.float32)
    share = summed_on_arrival(down_part.astype(jnp.bfloat16), "tp", 1)
    returned = share.astype(jnp.bfloat16).reshape(groups, row_count, share.shape[1])
    arrived = lax.all_to_all(returned, "ep", split_axis=0, concat_axis=0, tiled=True)
    part_total = jnp.sum(
        arrived.reshape(experts_n, SPREAD, cap, quarter).astype(jnp.float32), axis=1
    )
    expert_out = part_total.astype(jnp.bfloat16)
    expert_mix = jnp.dot(combine, expert_out.reshape(experts_n * cap, quarter).astype(jnp.float32))
    return (resid.astype(jnp.float32) + expert_mix).astype(jnp.bfloat16)


def solution(mesh):
    placed = (
        P("ep", None),
        P("ep"),
        P("ep", "tp", None, None),
        P(),
        P(None, "tp"),
        P(None, "tp"),
        P(None, "tp"),
        P("tp"),
        P("tp", None),
        P(),
        P("ep", None),
        P("ep", None),
        P("ep", None, "tp"),
        P("ep", None, "tp"),
        P("ep", "tp", None),
    )
    return jax.shard_map(body, mesh=mesh, in_specs=placed, out_specs=P("ep", "tp"), check_vma=False)
```

profile of v0, /device:TPU:1, one launch (start us, length us, event | category | flops | bytes accessed | tf_op | source)
XLA Modules:
  0.0 94.6 jit_solution(541615782359818185)
XLA Ops:
  0.0 0.0 copy-start
  0.0 0.0 copy-start.2
  0.0 0.0 copy-start.7
  0.0 0.0 copy-start.6
  0.0 0.0 copy-start.1
  0.0 0.0 copy-start.5
  0.1 0.8 convert_element_type.79
  0.9 1.0 %fusion.22 = f32[16]{0:T(128)S(1)} fusion(bf16[16,1024]{1,0:T(8,128)(2,1)} %param.15), kind=kLoop, calls=%fused_computation.35 | loop fusion | flops 49136 | bytes 32832 | tf_op jit(solution)/shard_map/reduce_sum | solution.py:74
  1.9 1.2 %fusion.10 = f32[16,1,128]{2,0,1:T(8,128)S(1)} fusion(bf16[1024,128]{1,0:T(8,128)(2,1)} %param.20, bf16[16,1024]{1,0:T(8,128)(2,1)} %param.15, f32[1024]{0:T(1024)} %param.18, f32[16]{0:T(128)S(1)} %add_rsqrt_fusion.2), kind=kOutput, calls=%fused_computation.18 | convolution fusion | flops 4263936 | bytes 307264 | tf_op jit(solution)/shard_map/dot_general | solution.py:77
  3.1 0.0 copy-start.3
  3.1 0.0 copy-start.4
  3.1 1.2 %fusion.8 = f32[16,1,128]{2,0,1:T(8,128)S(1)} fusion(bf16[1024,128]{1,0:T(8,128)(2,1)} %param.19, bf16[16,1024]{1,0:T(8,128)(2,1)} %param.15, f32[1024]{0:T(1024)} %param.18, f32[16]{0:T(128)S(1)} %add_rsqrt_fusion.2), kind=kOutput, calls=%fused_computation.16 | convolution fusion | flops 4263936 | bytes 307264 | tf_op jit(solution)/shard_map/dot_general | solution.py:76
  4.3 0.1 fusion.37
  4.5 0.2 fusion.45
  4.6 0.0 copy-done
  4.6 0.3 fusion.60
  4.9 0.0 copy-done.2
  4.9 0.0 copy-done.7
  4.9 0.0 copy-done.6
  4.9 0.3 fusion.59
  5.3 0.2 multiply_reduce_fusion.1
  5.5 0.0 copy-done.1
  5.5 0.0 copy-done.5
  5.5 0.2 convolution_convert_fusion.2
  5.7 0.7 broadcast_in_dim.4
  6.4 4.8 %all-to-all-start = ((bf16[4,16,1024]{2,1,0:T(8,128)(2,1)}), bf16[4,16,1024]{2,1,0:T(8,128)(2,1)S(1)}, u32[]{:S(2)}, u32[]{:S(2)}) async-start(bf16[4,16,1024]{2,1,0:T(8,128)(2,1)} %broadcast_in_dim.4), calls=%async_computation | async-start | bytes 262144 | tf_op jit(solution)/shard_map/all_to_all | solution.py:27
  11.2 0.0 copy-done.3
  11.2 0.0 copy-done.4
  11.2 0.1 copy.41
  11.3 0.1 eq.29
  11.4 0.1 fusion.28
  11.5 0.1 reduce_window_sum.11
  11.6 0.2 select_reduce_fusion.1
  11.7 0.1 reduce_sum.122
  11.8 0.1 copy.42
  11.9 0.8 dynamic-slice
  12.7 0.1 convert_reduce_fusion.1
  12.8 3.2 %all-to-all-done = bf16[4,16,1024]{2,1,0:T(8,128)(2,1)S(1)} async-done(((bf16[4,16,1024]{2,1,0:T(8,128)(2,1)}), bf16[4,16,1024]{2,1,0:T(8,128)(2,1)S(1)}, u32[]{:S(2)}, u32[]{:S(2)}) %all-to-all-start) | async-done | bytes 131104 | tf_op jit(solution)/shard_map/all_to_all | solution.py:27
  16.0 0.1 multiply_reduce_fusion
  16.2 0.2 convolution_convert_fusion.1
  16.4 0.1 broadcast_in_dim.5
  16.5 31.5 %all_to_all.20 = bf16[128,2,256]{2,1,0:T(2,128)(2,1)S(1)} all-to-all(bf16[128,2,256]{2,1,0:T(2,128)(2,1)S(1)} %bitcast.62), channel_id=1, replica_groups=mesh['ep'=128,'tp'=4] {'ep'}, dimensions={0} | all-to-all | bytes 262144 | tf_op jit(solution)/shard_map/all_to_all | solution.py:128
  48.0 9.7 %all_gather.3 = bf16[128,2,1024]{2,1,0:T(2,128)(2,1)S(1)} all-gather(bf16[128,2,256]{2,1,0:T(2,128)(2,1)S(1)} %all_to_all.20), channel_id=1, replica_groups=mesh['ep'=128,'tp'=4] {'tp'}, dimensions={2}, use_global_device_ids=true | all-gather | bytes 655360 | tf_op jit(solution)/shard_map/all_gather | solution.py:130
  57.8 0.2 reshape.276
  58.0 2.4 %fusion.14 = f32[256,448]{0,1:T(8,128)} fusion(bf16[256,1024]{1,0:T(8,128)(2,1)S(1)} %reshape.276, bf16[1,1024,448]{1,2,0:T(8,128)(2,1)} %param.27), kind=kOutput, calls=%fused_computation.21 | convolution fusion | flops 234881024 | bytes 1900544 | tf_op jit(solution)/shard_map/dot_general | solution.py:133
  60.4 2.9 %convolution_convert_fusion = bf16[256,1024]{1,0:T(8,128)(2,1)S(1)} fusion(bf16[256,1024]{1,0:T(8,128)(2,1)S(1)} %reshape.276, bf16[1,448,1024]{2,1,0:T(8,128)(2,1)} %param.29, bf16[1,1024,448]{1,2,0:T(8,128)(2,1)} %param.28, f32[256,448]{0,1:T(8,128)} %fusion.14), kind=kOutput, calls=%fused_computation.2 | convolution fusion | flops 470712320 | bytes 3342336 | tf_op jit(solution)/shard_map/dot_general | solution.py:136
  63.3 9.6 %all_to_all.21 = bf16[4,256,256]{2,1,0:T(8,128)(2,1)S(1)} all-to-all(bf16[4,256,256]{2,1,0:T(8,128)(2,1)S(1)} %bitcast.60), channel_id=1, replica_groups=mesh['ep'=128,'tp'=4] {'tp'}, dimensions={0} | all-to-all | bytes 1048576 | tf_op jit(solution)/shard_map/all_to_all | solution.py:21
  72.9 0.1 reduce_sum.127
  73.0 0.1 reshape.278
  73.0 20.6 %all_to_all.22 = bf16[128,2,256]{2,1,0:T(2,128)(2,1)S(1)} all-to-all(bf16[128,2,256]{2,1,0:T(2,128)(2,1)S(1)} %reshape.278), channel_id=1, replica_groups=mesh['ep'=128,'tp'=4] {'ep'}, dimensions={0} | all-to-all | bytes 262144 | tf_op jit(solution)/shard_map/all_to_all | solution.py:139
  93.7 0.2 bitcast_reduce_fusion
  93.9 0.7 fusion.3
  (14 shorter events, 0.2 us)
Async XLA Ops:
  0.0 4.6 %copy-start = (f32[16,1,128,256]{3,2,1,0:T(8,128)S(1)}, f32[16,1,128,256]{3,2,1,0:T(8,128)}, u32[]{:S(2)}) copy-start(f32[16,1,128,256]{3,2,1,0:T(8,128)} %param.17) | copy-start | bytes 6291460
  0.0 4.9 %copy-start.2 = (bf16[16,1024]{1,0:T(8,128)(2,1)S(1)}, bf16[16,1024]{1,0:T(8,128)(2,1)}, u32[]{:S(2)}) copy-start(bf16[16,1024]{1,0:T(8,128)(2,1)} %param.15) | copy-start | bytes 98308
  0.0 4.9 %copy-start.7 = (f32[1024]{0:T(1024)S(1)}, f32[1024]{0:T(1024)}, u32[]{:S(2)}) copy-start(f32[1024]{0:T(1024)} %param.18) | copy-start | bytes 12292
  0.0 4.9 %copy-start.6 = (bf16[1024,256]{1,0:T(8,128)(2,1)S(1)}, bf16[1024,256]{1,0:T(8,128)(2,1)}, u32[]{:S(2)}) copy-start(bf16[1024,256]{1,0:T(8,128)(2,1)} %param.21) | copy-start | bytes 1572868
  0.0 5.4 %copy-start.1 = (bf16[256,1024]{1,0:T(8,128)(2,1)S(1)}, bf16[256,1024]{1,0:T(8,128)(2,1)}, u32[]{:S(2)}) copy-start(bf16[256,1024]{1,0:T(8,128)(2,1)} %param.23) | copy-start | bytes 1572868
  0.0 5.4 %copy-start.5 = (f32[256]{0:T(256)S(1)}, f32[256]{0:T(256)}, u32[]{:S(2)}) copy-start(f32[256]{0:T(256)} %param.22) | copy-start | bytes 3076
  3.1 8.1 %copy-start.3 = (f32[16,2]{0,1:T(2,128)S(1)}, f32[16,2]{0,1:T(2,128)}, u32[]{:S(2)}) copy-start(f32[16,2]{0,1:T(2,128)} %param.26) | copy-start | bytes 388
  3.1 8.2 %copy-start.4 = (s32[16,2]{0,1:T(2,128)S(1)}, s32[16,2]{0,1:T(2,128)}, u32[]{:S(2)}) copy-start(s32[16,2]{0,1:T(2,128)} %param.25) | copy-start | bytes 388
  6.4 9.7 %all-to-all-start = ((bf16[4,16,1024]{2,1,0:T(8,128)(2,1)}), bf16[4,16,1024]{2,1,0:T(8,128)(2,1)S(1)}, u32[]{:S(2)}, u32[]{:S(2)}) async-start(bf16[4,16,1024]{2,1,0:T(8,128)(2,1)} %broadcast_in_dim.4), calls=%async_computation | async-start | bytes 262144 | tf_op jit(solution)/shard_map/all_to_all | solution.py:27
where the time goes:
time: 95 us; the launch traced here: 94.6 us
  blocking collectives  71.5 us (75%)
  matrix products  9.44 us (10%)
  starting transfers between devices  4.83 us (5%)
  waiting for transfers between devices  3.24 us (3%)
  other arithmetic  3.14 us (3%)
  local copies, waits for them, and re-layouts  2.24 us (2%)
    all_to_all x1, blocking collectives, body(): lax.all_to_all(send_buffer, 'ep', split_axis=0, concat_axis=0, tiled=True)  31.5 us
    all_to_all x1, blocking collectives, body(): lax.all_to_all(returned, 'ep', split_axis=0, concat_axis=0, tiled=True)  20.6 us
    all_gather x1, blocking collectives, body(): piece_cols = lax.all_gather(received, 'tp', axis=2, tiled=True)  9.74 us
    all_to_all x1, blocking collectives, summed_on_arrival(): lax.all_to_all(pieces, axis, split_axis=0, concat_axis=0, tiled=True)  9.56 us
    all_to_all x1, starting transfers between devices, copy_for_each(): return lax.all_to_all(copies, axis, split_axis=0, concat_axis=0, tiled=True)  4.83 us
    all_to_all x1, waiting for transfers between devices, copy_for_each(): return lax.all_to_all(copies, axis, split_axis=0, concat_axis=0, tiled=True)  3.24 us
    dot_general x1, matrix products, body(): down_part = jnp.dot(hidden, down_rows, preferred_element_type=jnp.float32)  2.9 us
    dot_general x1, matrix products, body(): gate_sum = jnp.dot(flat_in, gate_rows, preferred_element_type=jnp.float32)  2.4 us
  transfers between devices with their start and end apart: 1, of which 1 were waited for; matrix products, arithmetic and copies ran while one was open for 2% of the time, Pallas kernels for 0%

commit v1 on v0

--- a/solution.py
+++ b/solution.py
@@ -127,7 +127,9 @@
     send_buffer = jnp.repeat(packed, SPREAD, axis=0)
     received = lax.all_to_all(send_buffer, "ep", split_axis=0, concat_axis=0, tiled=True)
     groups, row_count, cols = received.shape
-    piece_cols = lax.all_gather(received, "tp", axis=2, tiled=True)
+    piece_cols = jnp.concatenate(
+        jax.lax.all_to_all(jnp.stack([received] * jax.lax.psum(1, "tp")), "tp", 0, 0), axis=2
+    )
     piece_width = piece_cols.shape[2]
     flat_in = piece_cols.reshape(groups * row_count, piece_width)
     gate_sum = jnp.dot(flat_in, gate_rows, preferred_element_type=jnp.float32)

time: 95 us -> 96.7 us (1.018)
  blocking collectives: 71.5 us -> 73.4 us
  matrix products: 9.44 us -> 8.25 us
    all_to_all x0 -> x1, blocking collectives: none -> 11.6 us  [body(): jax.lax.all_to_all(jnp.stack([received] * jax.lax.psum(1, 'tp')), 'tp', 0...]
    all_gather x1 -> x0, blocking collectives: 9.74 us -> none  [body(): piece_cols = lax.all_gather(received, 'tp', axis=2, tiled=True)]
    dot_general x1, matrix products: 2.4 us -> 1.21 us  [body(): gate_sum = jnp.dot(flat_in, gate_rows, preferred_element_type=jnp.float32)]
    all_to_all x1, blocking collectives: 9.56 us -> 10.7 us  [summed_on_arrival(): lax.all_to_all(pieces, axis, split_axis=0, concat_axis=0, tiled=True)]
    all_to_all x1, blocking collectives: 20.6 us -> 19.5 us  [body(): lax.all_to_all(returned, 'ep', split_axis=0, concat_axis=0, tiled=True)]
where the time goes in v1:
time: 96.7 us; the launch traced here: 96.3 us
  blocking collectives  73.4 us (76%)
  matrix products  8.25 us (9%)
  starting transfers between devices  4.83 us (5%)
  waiting for transfers between devices  3.24 us (3%)
  other arithmetic  3.14 us (3%)
  local copies, waits for them, and re-layouts  3.1 us (3%)
    all_to_all x1, blocking collectives, body(): lax.all_to_all(send_buffer, 'ep', split_axis=0, concat_axis=0, tiled=True)  31.7 us
    all_to_all x1, blocking collectives, body(): lax.all_to_all(returned, 'ep', split_axis=0, concat_axis=0, tiled=True)  19.5 us
    all_to_all x1, blocking collectives, body(): jax.lax.all_to_all(jnp.stack([received] * jax.lax.psum(1, 'tp')), 'tp', 0...  11.6 us
    all_to_all x1, blocking collectives, summed_on_arrival(): lax.all_to_all(pieces, axis, split_axis=0, concat_axis=0, tiled=True)  10.7 us
    all_to_all x1, starting transfers between devices, copy_for_each(): return lax.all_to_all(copies, axis, split_axis=0, concat_axis=0, tiled=True)  4.83 us
    all_to_all x1, waiting for transfers between devices, copy_for_each(): return lax.all_to_all(copies, axis, split_axis=0, concat_axis=0, tiled=True)  3.24 us
    dot_general x1, matrix products, body(): down_part = jnp.dot(hidden, down_rows, preferred_element_type=jnp.float32)  2.9 us
  transfers between devices with their start and end apart: 1, of which 1 were waited for; matrix products, arithmetic and copies ran while one was open for 2% of the time, Pallas kernels for 0%

profile of v1, /device:TPU:1, one launch (start us, length us, event | category | flops | bytes accessed | tf_op | source)
XLA Modules:
  0.0 96.3 jit_solution(12211598417894578315)
XLA Ops:
  0.0 0.0 copy-start
  0.0 0.0 copy-start.3
  0.0 0.0 copy-start.8
  0.0 0.0 copy-start.7
  0.0 0.0 copy-start.2
  0.0 0.0 copy-start.6
  0.1 0.8 convert_element_type.79
  0.9 1.0 %fusion.22 = f32[16]{0:T(128)S(1)} fusion(bf16[16,1024]{1,0:T(8,128)(2,1)} %param.15), kind=kLoop, calls=%fused_computation.35 | loop fusion | flops 49136 | bytes 32832 | tf_op jit(solution)/shard_map/reduce_sum | solution.py:74
  1.9 1.2 %fusion.10 = f32[16,1,128]{2,0,1:T(8,128)S(1)} fusion(bf16[1024,128]{1,0:T(8,128)(2,1)} %param.20, bf16[16,1024]{1,0:T(8,128)(2,1)} %param.15, f32[1024]{0:T(1024)} %param.18, f32[16]{0:T(128)S(1)} %add_rsqrt_fusion.2), kind=kOutput, calls=%fused_computation.18 | convolution fusion | flops 4263936 | bytes 307264 | tf_op jit(solution)/shard_map/dot_general | solution.py:77
  3.1 0.0 copy-start.4
  3.1 0.0 copy-start.5
  3.1 1.2 %fusion.8 = f32[16,1,128]{2,0,1:T(8,128)S(1)} fusion(bf16[1024,128]{1,0:T(8,128)(2,1)} %param.19, bf16[16,1024]{1,0:T(8,128)(2,1)} %param.15, f32[1024]{0:T(1024)} %param.18, f32[16]{0:T(128)S(1)} %add_rsqrt_fusion.2), kind=kOutput, calls=%fused_computation.16 | convolution fusion | flops 4263936 | bytes 307264 | tf_op jit(solution)/shard_map/dot_general | solution.py:76
  4.3 0.1 fusion.37
  4.5 0.2 fusion.45
  4.6 0.0 copy-done
  4.6 0.3 fusion.60
  4.9 0.0 copy-done.3
  4.9 0.0 copy-done.8
  4.9 0.0 copy-done.7
  4.9 0.3 fusion.59
  5.3 0.2 multiply_reduce_fusion.1
  5.5 0.0 copy-done.2
  5.5 0.0 copy-done.6
  5.5 0.2 convolution_convert_fusion.2
  5.7 0.7 broadcast_in_dim.4
  6.4 4.8 %all-to-all-start = ((bf16[4,16,1024]{2,1,0:T(8,128)(2,1)}), bf16[4,16,1024]{2,1,0:T(8,128)(2,1)S(1)}, u32[]{:S(2)}, u32[]{:S(2)}) async-start(bf16[4,16,1024]{2,1,0:T(8,128)(2,1)} %broadcast_in_dim.4), calls=%async_computation | async-start | bytes 262144 | tf_op jit(solution)/shard_map/all_to_all | solution.py:27
  11.2 0.0 copy-done.4
  11.2 0.0 copy-done.5
  11.2 0.1 copy.44
  11.3 0.1 eq.29
  11.4 0.1 fusion.28
  11.5 0.1 reduce_window_sum.11
  11.6 0.2 select_reduce_fusion.1
  11.7 0.1 reduce_sum.122
  11.8 0.1 copy.45
  11.9 0.8 dynamic-slice
  12.7 0.1 convert_reduce_fusion.1
  12.8 3.2 %all-to-all-done = bf16[4,16,1024]{2,1,0:T(8,128)(2,1)S(1)} async-done(((bf16[4,16,1024]{2,1,0:T(8,128)(2,1)}), bf16[4,16,1024]{2,1,0:T(8,128)(2,1)S(1)}, u32[]{:S(2)}, u32[]{:S(2)}) %all-to-all-start) | async-done | bytes 131104 | tf_op jit(solution)/shard_map/all_to_all | solution.py:27
  16.0 0.1 multiply_reduce_fusion
  16.2 0.2 convolution_convert_fusion.1
  16.4 0.0 copy-start.1
  16.4 0.1 broadcast_in_dim.5
  16.5 31.7 %all_to_all.25 = bf16[128,2,256]{2,1,0:T(2,128)(2,1)S(1)} all-to-all(bf16[128,2,256]{2,1,0:T(2,128)(2,1)S(1)} %bitcast.70), channel_id=1, replica_groups=mesh['ep'=128,'tp'=4] {'ep'}, dimensions={0} | all-to-all | bytes 262144 | tf_op jit(solution)/shard_map/all_to_all | solution.py:128
  48.2 0.3 stack.2
  48.5 11.6 %all_to_all.26 = bf16[4,128,2,256]{3,2,1,0:T(2,128)(2,1)S(1)} all-to-all(bf16[4,128,2,256]{3,2,1,0:T(2,128)(2,1)S(1)} %stack.2), channel_id=1, replica_groups=mesh['ep'=128,'tp'=4] {'tp'}, dimensions={0} | all-to-all | bytes 1048576 | tf_op jit(solution)/shard_map/all_to_all | solution.py:131
  60.0 0.7 copy.46
  60.7 0.1 copy.54
  60.8 0.0 copy-done.1
  60.8 1.2 %fusion.14 = f32[256,448]{0,1:T(8,128)} fusion(bf16[256,1024]{1,0:T(8,128)(2,1)S(1)} %bitcast.67, bf16[1,1024,448]{1,2,0:T(8,128)(2,1)S(1)} %copy-done.1), kind=kOutput, calls=%fused_computation.21 | convolution fusion | flops 234881024 | bytes 1900544 | tf_op jit(solution)/shard_map/dot_general | solution.py:135
  62.1 2.9 %convolution_convert_fusion = bf16[256,1024]{1,0:T(8,128)(2,1)S(1)} fusion(bf16[256,1024]{1,0:T(8,128)(2,1)S(1)} %bitcast.68, bf16[1,448,1024]{2,1,0:T(8,128)(2,1)} %param.29, bf16[1,1024,448]{1,2,0:T(8,128)(2,1)} %param.28, f32[256,448]{0,1:T(8,128)} %fusion.14), kind=kOutput, calls=%fused_computation.2 | convolution fusion | flops 470712320 | bytes 3342336 | tf_op jit(solution)/shard_map/dot_general | solution.py:138
  65.0 10.7 %all_to_all.27 = bf16[4,256,256]{2,1,0:T(8,128)(2,1)S(1)} all-to-all(bf16[4,256,256]{2,1,0:T(8,128)(2,1)S(1)} %bitcast.66), channel_id=1, replica_groups=mesh['ep'=128,'tp'=4] {'tp'}, dimensions={0} | all-to-all | bytes 1048576 | tf_op jit(solution)/shard_map/all_to_all | solution.py:21
  75.7 0.1 reduce_sum.127
  75.8 0.1 reshape.280
  75.9 19.5 %all_to_all.28 = bf16[128,2,256]{2,1,0:T(2,128)(2,1)S(1)} all-to-all(bf16[128,2,256]{2,1,0:T(2,128)(2,1)S(1)} %reshape.280), channel_id=1, replica_groups=mesh['ep'=128,'tp'=4] {'ep'}, dimensions={0} | all-to-all | bytes 262144 | tf_op jit(solution)/shard_map/all_to_all | solution.py:141
  95.3 0.2 bitcast_reduce_fusion
  95.5 0.7 fusion.3
  (14 shorter events, 0.2 us)
Async XLA Ops:
  0.0 4.6 %copy-start = (f32[16,1,128,256]{3,2,1,0:T(8,128)S(1)}, f32[16,1,128,256]{3,2,1,0:T(8,128)}, u32[]{:S(2)}) copy-start(f32[16,1,128,256]{3,2,1,0:T(8,128)} %param.17) | copy-start | bytes 6291460
  0.0 4.9 %copy-start.3 = (bf16[16,1024]{1,0:T(8,128)(2,1)S(1)}, bf16[16,1024]{1,0:T(8,128)(2,1)}, u32[]{:S(2)}) copy-start(bf16[16,1024]{1,0:T(8,128)(2,1)} %param.15) | copy-start | bytes 98308
  0.0 4.9 %copy-start.8 = (f32[1024]{0:T(1024)S(1)}, f32[1024]{0:T(1024)}, u32[]{:S(2)}) copy-start(f32[1024]{0:T(1024)} %param.18) | copy-start | bytes 12292
  0.0 4.9 %copy-start.7 = (bf16[1024,256]{1,0:T(8,128)(2,1)S(1)}, bf16[1024,256]{1,0:T(8,128)(2,1)}, u32[]{:S(2)}) copy-start(bf16[1024,256]{1,0:T(8,128)(2,1)} %param.21) | copy-start | bytes 1572868
  0.0 5.4 %copy-start.2 = (bf16[256,1024]{1,0:T(8,128)(2,1)S(1)}, bf16[256,1024]{1,0:T(8,128)(2,1)}, u32[]{:S(2)}) copy-start(bf16[256,1024]{1,0:T(8,128)(2,1)} %param.23) | copy-start | bytes 1572868
  0.0 5.4 %copy-start.6 = (f32[256]{0:T(256)S(1)}, f32[256]{0:T(256)}, u32[]{:S(2)}) copy-start(f32[256]{0:T(256)} %param.22) | copy-start | bytes 3076
  3.1 8.1 %copy-start.4 = (f32[16,2]{0,1:T(2,128)S(1)}, f32[16,2]{0,1:T(2,128)}, u32[]{:S(2)}) copy-start(f32[16,2]{0,1:T(2,128)} %param.26) | copy-start | bytes 388
  3.1 8.2 %copy-start.5 = (s32[16,2]{0,1:T(2,128)S(1)}, s32[16,2]{0,1:T(2,128)}, u32[]{:S(2)}) copy-start(s32[16,2]{0,1:T(2,128)} %param.25) | copy-start | bytes 388
  6.4 9.7 %all-to-all-start = ((bf16[4,16,1024]{2,1,0:T(8,128)(2,1)}), bf16[4,16,1024]{2,1,0:T(8,128)(2,1)S(1)}, u32[]{:S(2)}, u32[]{:S(2)}) async-start(bf16[4,16,1024]{2,1,0:T(8,128)(2,1)} %broadcast_in_dim.4), calls=%async_computation | async-start | bytes 262144 | tf_op jit(solution)/shard_map/all_to_all | solution.py:27
  16.4 44.4 %copy-start.1 = (bf16[1,1024,448]{1,2,0:T(8,128)(2,1)S(1)}, bf16[1,1024,448]{1,2,0:T(8,128)(2,1)}, u32[]{:S(2)}) copy-start(bf16[1,1024,448]{1,2,0:T(8,128)(2,1)} %param.27) | copy-start | bytes 2752516
